TPU v7x, 512 devices: a whole 4x8x8 slice. The times are simulated.
512 devices in a mesh: ep: 32 (over z, x), tp: 16 (over y, core).
Axes of the slice: x: 4, y: 8, z: 8, core: 2. Of those that a mesh axis runs over, the one named last changes fastest.
Arguments:
- conv_value: bfloat16 [16384, 2048], P('ep', 'tp'), may hold values from -6 to 6
- conv_gate: bfloat16 [16384, 2048], P('ep', 'tp'), may hold values from -9 to 9
- conv_taps: float32 [31, 2048], P(None, 'tp'), may hold values from -14 to 14
- norm_gain: float32 [2048], P('tp'), may hold values from 0.1 to 1.9
- norm_shift: float32 [2048], P('tp'), may hold values from -3 to 3
- conv_out_weight: bfloat16 [2048, 2048], P(None, 'tp'), may hold values from -0.125 to 0.125
- moe_input: bfloat16 [4096, 2048], P('ep'), may hold values from -6 to 6
- moe_gain: float32 [2048], replicated, may hold values from 0.1 to 1.9
- routes: int32 [4096, 4], P('ep'), may hold values from 0 to 31, all different within a row; in each aligned block of 128 rows (0 to 127, 128 to 255, ...) at most 32 rows name the same one
- route_weights: float32 [4096, 4], P('ep'), may hold values from 0.25 to 1
- expert_gate: bfloat16 [32, 2048, 4096], P('ep', None, 'tp'), may hold values from -0.125 to 0.125
- expert_up: bfloat16 [32, 2048, 4096], P('ep', None, 'tp'), may hold values from -0.125 to 0.125
- expert_down: bfloat16 [32, 4096, 2048], P('ep', None, 'tp'), may hold values from -0.09375 to 0.09375
- shared_gate: bfloat16 [2048, 512], P(None, 'tp'), may hold values from -0.125 to 0.125
- shared_up: bfloat16 [2048, 512], P(None, 'tp'), may hold values from -0.125 to 0.125
- shared_down: bfloat16 [512, 2048], P(None, 'tp'), may hold values from -0.25 to 0.25
Outputs:
- conv_result: bfloat16 [16384, 2048], P('ep', 'tp')
- moe_result: bfloat16 [4096, 2048], P('ep', 'tp')
Inputs may be any that keep to these rules, and one draw needn't show every extreme that they name: `routes`: in the rows of one device (aligned blocks of 128 rows) no expert is named by more than 32 rows, a bound that some block reaches; each row names 4 different experts.
All inputs are finite; a program needn't handle non-finite values.
Results may differ from a plain program's by a relative error of at most 0.0068.
Values may be sent and summed in bfloat16 or wider, within the bound.
A program may use at most 64 MiB of HBM per device.

v0:
```python
import jax
import jax.numpy as jnp
from jax import lax
from jax.sharding import Mesh
from jax.sharding import PartitionSpec as P

EP = ("ep_0", "ep_1")


def from_behind(value, axis, steps):
    count = lax.axis_size(axis)
    initial, last = (max(0, -steps), min(count, count - steps))
    return lax.ppermute(value, axis, [(source, source + steps) for source in range(initial, last)])


def cut_along(array, dim, peers):
    before, after = (array.shape[:dim], array.shape[dim + 1 :])
    return jnp.moveaxis(array.reshape(*before, peers, -1, *after), dim, 0)


def joined_along(parts, dim):
    lengths = list(parts.shape[1:])
    lengths[dim] *= parts.shape[0]
    return jnp.moveaxis(parts, 0, dim).reshape(lengths)


def exchange_in_order(parts, axes, turns):
    lengths = [lax.axis_size(a) for a in axes]
    parts = parts.reshape(*lengths, *parts.shape[1:])
    for k in turns:
        parts = lax.all_to_all(parts, axes[k], split_axis=k, concat_axis=k, tiled=True)
    return parts.reshape(-1, *parts.shape[len(axes) :])


def stepwise_exchange(array, axes, turns, split_dim, concat_dim):
    parts = cut_along(array, split_dim, lax.axis_size(axes))
    return joined_along(exchange_in_order(parts, axes, turns), concat_dim)


def body(
    conv_value,
    conv_gate,
    conv_taps,
    norm_gain,
    norm_shift,
    conv_out_weight,
    moe_input,
    moe_gain,
    routes,
    route_weights,
    expert_gate,
    expert_up,
    expert_down,
    shared_gate,
    shared_up,
    shared_down,
):
    tap_count = conv_taps.shape[0]
    rows_a = conv_value.shape[0]
    glu_rows = (
        conv_value.astype(jnp.float32) * jax.nn.sigmoid(conv_gate.astype(jnp.float32))
    ).astype(jnp.bfloat16)
    before = from_behind(glu_rows[rows_a - (tap_count - 1) :], EP, 1)
    padded = jnp.concatenate([before, glu_rows], axis=0)
    filtered = jnp.zeros(glu_rows.shape, jnp.float32)
    for offset in range(tap_count):
        filtered = filtered + conv_taps[offset] * padded[offset : offset + rows_a].astype(
            jnp.float32
        )
    row_total, squares = lax.psum(
        (jnp.sum(filtered, axis=1), jnp.sum(filtered * filtered, axis=1)), "tp"
    )
    channels = conv_out_weight.shape[0]
    row_mean = row_total / channels
    row_square = squares / channels
    scaled = (filtered - row_mean[:, None]) * lax.rsqrt(row_square - row_mean * row_mean + 1e-05)[
        :, None
    ]
    conv_hidden = jax.nn.silu(scaled * norm_gain + norm_shift).astype(jnp.bfloat16)
    conv_sum = jnp.dot(
        lax.all_gather(conv_hidden, "tp", axis=1, tiled=True),
        conv_out_weight,
        preferred_element_type=jnp.float32,
    )
    conv_result = conv_sum.astype(jnp.bfloat16)
    inputs = moe_input.astype(jnp.float32)
    normed = (
        inputs * lax.rsqrt(jnp.mean(inputs * inputs, axis=1, keepdims=True) + 1e-06) * moe_gain
    ).astype(jnp.bfloat16)
    rows_b, per_row = routes.shape
    model_width = normed.shape[1]
    groups = lax.axis_size(EP)
    capacity = 2 * rows_b * per_row // groups
    flat_expert = routes.reshape(-1)
    owner_row = jnp.arange(rows_b * per_row, dtype=jnp.int32) // per_row
    expert_hits = (flat_expert[:, None] == jnp.arange(groups, dtype=jnp.int32)[None, :]).astype(
        jnp.int32
    )
    slot_rank = jnp.sum((jnp.cumsum(expert_hits, axis=0) - expert_hits) * expert_hits, axis=1)
    slot_index = flat_expert * capacity + slot_rank
    outgoing = (
        jnp.zeros((groups * capacity, model_width), jnp.bfloat16)
        .at[slot_index]
        .set(normed[owner_row])
    )
    outgoing = outgoing.reshape(groups, capacity, model_width)
    slot_share = capacity // lax.axis_size("tp")
    own_slots = lax.dynamic_slice_in_dim(outgoing, lax.axis_index("tp") * slot_share, slot_share, 1)
    partial_rows = lax.all_to_all(own_slots, EP, split_axis=0, concat_axis=0, tiled=True)
    arrived = lax.all_gather(partial_rows, "tp", axis=1, tiled=True)
    arrived_rows = arrived.reshape(groups * capacity, model_width)
    gate_value = jnp.dot(arrived_rows, expert_gate[0], preferred_element_type=jnp.float32)
    upward = jnp.dot(arrived_rows, expert_up[0], preferred_element_type=jnp.float32)
    expert_hidden = (jax.nn.silu(gate_value) * upward).astype(jnp.bfloat16)
    shared_hidden = (
        jax.nn.silu(jnp.dot(normed, shared_gate, preferred_element_type=jnp.float32))
        * jnp.dot(normed, shared_up, preferred_element_type=jnp.float32)
    ).astype(jnp.bfloat16)
    columns = expert_down.shape[2]
    routed_rows = expert_down[0]
    routed_sum = jnp.dot(
        lax.all_gather(expert_hidden, "tp", axis=1, tiled=True),
        routed_rows,
        preferred_element_type=jnp.float32,
    )
    shared_sum = jnp.dot(
        lax.all_gather(shared_hidden, "tp", axis=1, tiled=True),
        shared_down,
        preferred_element_type=jnp.float32,
    )
    expert_out = routed_sum.astype(jnp.bfloat16).reshape(groups, capacity, columns)
    returned = stepwise_exchange(expert_out, EP, (0, 1), 0, 0).reshape(groups * capacity, columns)
    picked = returned[slot_index].astype(jnp.float32) * route_weights.reshape(-1)[:, None]
    moe_sum = jnp.sum(picked.reshape(rows_b, per_row, columns), axis=1) + shared_sum
    return (conv_result, moe_sum.astype(jnp.bfloat16))


def solution(mesh):
    finer = Mesh(mesh.devices.reshape(8, 4, mesh.shape["tp"]), ("ep_0", "ep_1", "tp"))
    in_specs = (
        P(EP, "tp"),
        P(EP, "tp"),
        P(None, "tp"),
        P("tp"),
        P("tp"),
        P(None, "tp"),
        P(EP, None),
        P(),
        P(EP, None),
        P(EP, None),
        P(EP, None, "tp"),
        P(EP, None, "tp"),
        P(EP, None, "tp"),
        P(None, "tp"),
        P(None, "tp"),
        P(None, "tp"),
    )
    out_specs = (P(EP, "tp"), P(EP, "tp"))
    return jax.shard_map(body, mesh=finer, in_specs=in_specs, out_specs=out_specs, check_vma=False)
```

profile of v0, /device:TPU:1, one launch (start us, length us, event | category | flops | bytes accessed | tf_op | source)
XLA Modules:
  0.0 226.3 jit_solution(18367188397835349781)
XLA Ops:
  7.2 0.0 copy-start
  7.2 0.0 all-gather.6.cloned.1.call-start
  7.2 0.8 broadcast_multiply_fusion
  8.0 0.8 copy.33
  8.8 0.1 eq.29
  8.9 0.1 eq.25
  9.0 1.2 fusion.6
  10.3 0.1 copy.32
  10.4 0.1 mul.506
  10.5 1.2 reduce-window.6
  11.7 0.2 slice_reduce_fusion
  11.9 0.1 fusion.45
  12.1 1.2 fusion.8
  13.3 12.8 %scatter_custom_fusion = bf16[1024,2048]{1,0:T(8,128)(2,1)} fusion(s32[512]{0:T(512)S(1)} %bitcast.118, bf16[128,2048]{1,0:T(8,128)(2,1)S(1)} %fusion.8, s32[1024]{0:T(1024)S(1)} %pad_clamp_fusion.1, bf16[]{:T(256)} %constant.47.clone.1), kind=kCustom, calls=%fused_computation.3 | custom fusion | bytes 4194306 | tf_op jit(solution)/shard_map/scatter | solution.py:104
  26.1 1.5 constant_dynamic-slice_fusion
  27.6 24.8 %all_to_all.15 = bf16[32,2,2048]{2,1,0:T(2,128)(2,1)S(1)} all-to-all(bf16[32,2,2048]{2,1,0:T(2,128)(2,1)S(1)} %constant_dynamic-slice_fusion), channel_id=1, replica_groups=mesh['ep_0'=8,'ep_1'=4,'tp'=16] {'ep_0','ep_1'}, dimensions={0} | all-to-all | bytes 524288 | tf_op jit(solution)/shard_map/all_to_all | solution.py:109
  52.4 0.8 copy.36
  53.2 0.0 all-gather.6.cloned.1.call-update
  53.2 0.0 all-gather.8.cloned.1.call-start
  53.3 42.1 %all-gather.6.cloned.1.call-done = bf16[32,32,2048]{2,0,1:T(8,128)(2,1)} async-done(((bf16[32,2,2048]{2,0,1:T(8,128)(2,1)}), bf16[32,32,2048]{2,0,1:T(8,128)(2,1)}) %all-gather.6.cloned.1.call-update) | async-done | bytes 4194320 | tf_op jit(solution)/shard_map/all_gather | solution.py:110
  95.4 4.5 %copy.37 = bf16[32,32,2048]{2,1,0:T(8,128)(2,1)S(1)} copy(bf16[32,32,2048]{2,0,1:T(8,128)(2,1)} %all-gather.6.cloned.1.call-done) | data formatting | bytes 8388608 | tf_op jit(solution)/shard_map/all_gather | solution.py:110
  99.9 0.0 copy-start.11
  99.9 0.0 copy-done
  99.9 1.3 fusion.11
  101.2 0.0 copy-done.11
  101.2 0.0 copy-start.2
  101.2 0.0 copy-start.3
  101.2 0.0 copy-start.7
  101.2 0.0 copy-start.9
  101.2 0.0 copy-start.10
  101.2 2.1 fusion.3
  103.4 0.0 all-gather.8.cloned.1.call-update
  103.4 0.0 all-gather.4.cloned.1.call-start
  103.4 0.1 multiply_convert_fusion.1
  103.5 3.1 %collective-permute-start = (bf16[30,128]{1,0:T(8,128)(2,1)S(1)}, bf16[30,128]{1,0:T(8,128)(2,1)S(1)}, u32[]{:S(2)}, u32[]{:S(2)}) collective-permute-start(bf16[30,128]{1,0:T(8,128)(2,1)S(1)} %slice.260), channel_id=1, source_target_pairs={{0,16},{16,32},{32,48},{48,64},{64,80},{80,96},{96,112},{112,128},... | collective-permute-start | bytes 23048 | tf_op jit(solution)/shard_map/ppermute | solution.py:13
  106.6 0.0 copy-done.7
  106.7 0.7 collective-permute-done
  107.4 1.2 fusion.47
  108.6 25.0 %all-reduce = (f32[512]{0:T(512)S(1)}, f32[512]{0:T(512)S(1)}) all-reduce(f32[512]{0:T(512)S(1)} %get-tuple-element.3, f32[512]{0:T(512)S(1)} %get-tuple-element.2), channel_id=1, replica_groups=mesh['ep_0'=8,'ep_1'=4,'tp'=16] {'tp'}, use_global_device_ids=true, to_apply=%region_3.0 | all-reduce | flops 1024 | bytes 8192 | tf_op jit(solution)/shard_map/psum | solution.py:70
  133.7 0.9 multiply_convert_fusion
  134.5 0.0 all-gather.4.cloned.1.call-update
  134.6 0.0 copy-start.4
  134.6 0.0 copy-start.8
  134.6 0.0 copy-start.5
  134.6 0.0 copy-start.1
  134.6 35.8 %all-gather.8.cloned.1.call-done = bf16[1024,4096]{1,0:T(8,128)(2,1)} async-done(((bf16[1024,256]{1,0:T(8,128)(2,1)}), bf16[1024,4096]{1,0:T(8,128)(2,1)}) %all-gather.8.cloned.1.call-update) | async-done | bytes 8388624 | tf_op jit(solution)/shard_map/all_gather | solution.py:122
  170.4 6.7 %convolution_convert_fusion = bf16[1024,128]{1,0:T(8,128)(2,1)} fusion(bf16[1024,4096]{1,0:T(8,128)(2,1)} %all-gather.8.cloned.1.call-done, bf16[1,4096,128]{2,1,0:T(8,128)(2,1)} %param.28), kind=kOutput, calls=%fused_computation.39 | convolution fusion | flops 1073872896 | bytes 9699328 | tf_op jit(solution)/shard_map/dot_general | solution.py:121
  177.1 6.5 %all-to-all-start.1 = ((bf16[8,4,1,32,128]{4,3,1,2,0:T(8,128)(2,1)}), bf16[8,4,1,32,128]{4,3,1,2,0:T(8,128)(2,1)S(1)}, u32[]{:S(2)}, u32[]{:S(2)}) async-start(bf16[8,4,1,32,128]{4,3,1,2,0:T(8,128)(2,1)} %bitcast.41), calls=%async_computation.1 | async-start | bytes 524288 | tf_op jit(solution)/shard_map/all_to_all | solution.py:31
  183.6 0.0 copy-done.4
  183.6 0.3 fusion.48
  183.9 0.0 copy-done.8
  183.9 0.1 copy.41
  184.1 0.0 copy-done.5
  184.1 0.3 fusion.5
  184.3 16.1 %all_gather.15 = bf16[128,512]{0,1:T(8,128)(2,1)S(1)} all-gather(bf16[128,32]{0,1:T(8,128)(2,1)S(1)} %fusion.5), channel_id=1, replica_groups=mesh['ep_0'=8,'ep_1'=4,'tp'=16] {'tp'}, dimensions={1}, use_global_device_ids=true | all-gather | bytes 139264 | tf_op jit(solution)/shard_map/all_gather | solution.py:127
  200.4 0.0 all-to-all-done.1
  200.4 0.7 copy.39
  201.1 4.1 %all-to-all-start.2 = ((bf16[8,4,1,32,128]{4,3,0,2,1:T(8,128)(2,1)}), bf16[8,4,1,32,128]{4,3,0,2,1:T(8,128)(2,1)S(1)}, u32[]{:S(2)}, u32[]{:S(2)}) async-start(bf16[8,4,1,32,128]{4,3,0,2,1:T(8,128)(2,1)} %copy.39), calls=%async_computation.2 | async-start | bytes 524288 | tf_op jit(solution)/shard_map/all_to_all | solution.py:31
  205.2 9.1 %all-gather.4.cloned.1.call-done = bf16[512,2048]{1,0:T(8,128)(2,1)} async-done(((bf16[512,128]{1,0:T(8,128)(2,1)}), bf16[512,2048]{1,0:T(8,128)(2,1)}) %all-gather.4.cloned.1.call-update) | async-done | bytes 2097168 | tf_op jit(solution)/shard_map/all_gather | solution.py:81
  214.3 3.0 %convolution_convert_fusion.1 = bf16[512,128]{1,0:T(8,128)(2,1)} fusion(bf16[512,2048]{1,0:T(8,128)(2,1)} %all-gather.4.cloned.1.call-done, bf16[2048,128]{1,0:T(8,128)(2,1)S(1)} %copy-done.1), kind=kOutput, calls=%fused_computation.40 | convolution fusion | flops 268500992 | bytes 2752512 | tf_op jit(solution)/shard_map/dot_general | solution.py:80
  217.2 0.0 all-to-all-done.2
  217.3 1.3 gather_fusion
  218.6 0.2 fusion.13
  218.9 0.8 fusion.4
  (20 shorter events, 0.2 us)
Async XLA Ops:
  7.2 92.7 %copy-start = (bf16[1,2048,256]{2,1,0:T(8,128)(2,1)S(1)}, bf16[1,2048,256]{2,1,0:T(8,128)(2,1)}, u32[]{:S(2)}) copy-start(bf16[1,2048,256]{2,1,0:T(8,128)(2,1)} %param.26) | copy-start | bytes 3145732
  7.2 88.2 %all-gather.6.cloned.1.call-start = ((), (), s32[]{:S(2)}) async-start(), calls=%async_computation.4 | async-start | bytes 4456448 | tf_op jit(solution)/shard_map/all_gather | solution.py:110
  53.2 117.2 %all-gather.8.cloned.1.call-start = ((), (), s32[]{:S(2)}) async-start(), calls=%async_computation.5 | async-start | bytes 8912896 | tf_op jit(solution)/shard_map/all_gather | solution.py:122
  99.9 1.3 copy-start.11
  101.2 2.3 copy-start.2
  101.2 2.3 copy-start.3
  101.2 5.5 %copy-start.7 = (f32[31,128]{1,0:T(8,128)S(1)}, f32[31,128]{1,0:T(8,128)}, u32[]{:S(2)}) copy-start(f32[31,128]{1,0:T(8,128)} %param.18) | copy-start | bytes 47620
  101.2 32.4 %copy-start.9 = (f32[128]{0:T(128)S(1)}, f32[128]{0:T(128)}, u32[]{:S(2)}) copy-start(f32[128]{0:T(128)} %param.20) | copy-start | bytes 1540
  101.2 32.4 %copy-start.10 = (f32[128]{0:T(128)S(1)}, f32[128]{0:T(128)}, u32[]{:S(2)}) copy-start(f32[128]{0:T(128)} %param.19) | copy-start | bytes 1540
  103.4 110.9 %all-gather.4.cloned.1.call-start = ((), (), s32[]{:S(2)}) async-start(), calls=%async_computation.3 | async-start | bytes 2228224 | tf_op jit(solution)/shard_map/all_gather | solution.py:81
  103.5 3.9 %collective-permute-start = (bf16[30,128]{1,0:T(8,128)(2,1)S(1)}, bf16[30,128]{1,0:T(8,128)(2,1)S(1)}, u32[]{:S(2)}, u32[]{:S(2)}) collective-permute-start(bf16[30,128]{1,0:T(8,128)(2,1)S(1)} %slice.260), channel_id=1, source_target_pairs={{0,16},{16,32},{32,48},{48,64},{64,80},{80,96},{96,112},{112,128},... | collective-permute-start | bytes 23048 | tf_op jit(solution)/shard_map/ppermute | solution.py:13
  134.6 49.1 %copy-start.4 = (bf16[2048,32]{0,1:T(8,128)(2,1)S(1)}, bf16[2048,32]{0,1:T(8,128)(2,1)}, u32[]{:S(2)}) copy-start(bf16[2048,32]{0,1:T(8,128)(2,1)} %param.29) | copy-start | bytes 393220
  134.6 49.3 %copy-start.8 = (f32[128,4]{0,1:T(4,128)S(1)}, f32[128,4]{0,1:T(4,128)}, u32[]{:S(2)}) copy-start(f32[128,4]{0,1:T(4,128)} %param.25) | copy-start | bytes 6148
  134.6 49.5 %copy-start.5 = (bf16[2048,32]{0,1:T(8,128)(2,1)S(1)}, bf16[2048,32]{0,1:T(8,128)(2,1)}, u32[]{:S(2)}) copy-start(bf16[2048,32]{0,1:T(8,128)(2,1)} %param.30) | copy-start | bytes 393220
  134.6 79.7 %copy-start.1 = (bf16[2048,128]{1,0:T(8,128)(2,1)S(1)}, bf16[2048,128]{1,0:T(8,128)(2,1)}, u32[]{:S(2)}) copy-start(bf16[2048,128]{1,0:T(8,128)(2,1)} %param.21) | copy-start | bytes 1572868
  177.1 41.8 %copy-start.6 = (bf16[512,128]{1,0:T(8,128)(2,1)S(1)}, bf16[512,128]{1,0:T(8,128)(2,1)}, u32[]{:S(2)}) copy-start(bf16[512,128]{1,0:T(8,128)(2,1)} %param.31) | copy-start | bytes 393220
  177.1 23.3 %all-to-all-start.1 = ((bf16[8,4,1,32,128]{4,3,1,2,0:T(8,128)(2,1)}), bf16[8,4,1,32,128]{4,3,1,2,0:T(8,128)(2,1)S(1)}, u32[]{:S(2)}, u32[]{:S(2)}) async-start(bf16[8,4,1,32,128]{4,3,1,2,0:T(8,128)(2,1)} %bitcast.41), calls=%async_computation.1 | async-start | bytes 524288 | tf_op jit(solution)/shard_map/all_to_all | solution.py:31
  201.1 16.1 %all-to-all-start.2 = ((bf16[8,4,1,32,128]{4,3,0,2,1:T(8,128)(2,1)}), bf16[8,4,1,32,128]{4,3,0,2,1:T(8,128)(2,1)S(1)}, u32[]{:S(2)}, u32[]{:S(2)}) async-start(bf16[8,4,1,32,128]{4,3,0,2,1:T(8,128)(2,1)} %copy.39), calls=%async_computation.2 | async-start | bytes 524288 | tf_op jit(solution)/shard_map/all_to_all | solution.py:31
Sparse Core Ops, SparseCore 0:
  53.3 42.0 all-gather.5
  103.5 66.8 all-gather.7
  173.1 41.1 all-gather.3
where the time goes:
time: 227 us; the launch traced here: 226 us
  waiting for transfers between devices  87.8 us (39%)
  blocking collectives  65.9 us (29%)
  local copies, waits for them, and re-layouts  23.3 us (10%)
  matrix products  14.4 us (6%)
  between operations  14 us (6%)
  starting transfers between devices  13.8 us (6%)
  other arithmetic  6.99 us (3%)
    all_gather x1, waiting for transfers between devices, body(): arrived = lax.all_gather(partial_rows, 'tp', axis=1, tiled=True)  42.1 us
    all_gather x1, waiting for transfers between devices, body(): lax.all_gather(expert_hidden, 'tp', axis=1, tiled=True)  35.8 us
    psum x1, blocking collectives, body(): lax.psum((jnp.sum(filtered, axis=1), jnp.sum(filtered * filtered, axis=1)...  25 us
    all_to_all x1, blocking collectives, body(): lax.all_to_all(own_slots, EP, split_axis=0, concat_axis=0, tiled=True)  24.8 us
    all_gather x1, blocking collectives, body(): lax.all_gather(shared_hidden, 'tp', axis=1, tiled=True)  16.1 us
    scatter x1, local copies, waits for them, and re-layouts, body(): outgoing = jnp.zeros((groups * capacity, model_width), jnp.bfloat16).at[s...  12.8 us
    all_to_all x2, starting transfers between devices, exchange_in_order(): lax.all_to_all(parts, axes[k], split_axis=k, concat_axis=k, tiled=True)  10.6 us
    all_gather x1, waiting for transfers between devices, body(): lax.all_gather(conv_hidden, 'tp', axis=1, tiled=True)  9.08 us
  transfers between devices with their start and end apart: 6, of which 4 were waited for; matrix products, arithmetic and copies ran while one was open for 6% of the time, Pallas kernels for 0%

commit v1 on v0

--- a/solution.py
+++ b/solution.py
@@ -5,6 +5,28 @@
 from jax.sharding import PartitionSpec as P
 
 EP = ("ep_0", "ep_1")
+
+
+def laid_out(blocks, dim):
+    shape = list(blocks.shape[1:])
+    shape[dim] *= blocks.shape[0]
+    return jnp.moveaxis(blocks, 0, dim).reshape(shape)
+
+
+def gather_around(x, axis, dim):
+    size = lax.axis_size(axis)
+    pairs = [(i, (i + 1) % size) for i in range(size)]
+    back = [(b, a) for a, b in pairs]
+    lower, upper = ([], [])
+    for step in range(size - 1):
+        if step % 2 == 0:
+            lower.append(lax.ppermute(lower[-1] if lower else x, axis, pairs))
+        else:
+            upper.append(lax.ppermute(upper[-1] if upper else x, axis, back))
+    blocks = jnp.stack([*lower[::-1], x, *upper])
+    shift = lax.axis_index(axis) - len(lower)
+    blocks = blocks[(jnp.arange(size) - shift) % size]
+    return laid_out(blocks, dim)
 
 
 def from_behind(value, axis, steps):
@@ -124,9 +146,7 @@
         preferred_element_type=jnp.float32,
     )
     shared_sum = jnp.dot(
-        lax.all_gather(shared_hidden, "tp", axis=1, tiled=True),
-        shared_down,
-        preferred_element_type=jnp.float32,
+        gather_around(shared_hidden, "tp", 1), shared_down, preferred_element_type=jnp.float32
     )
     expert_out = routed_sum.astype(jnp.bfloat16).reshape(groups, capacity, columns)
     returned = stepwise_exchange(expert_out, EP, (0, 1), 0, 0).reshape(groups * capacity, columns)

time: 227 us -> 227 us (level)
  starting transfers between devices: 13.8 us -> 36.2 us
  blocking collectives: 65.9 us -> 52.1 us
  waiting for transfers between devices: 87.8 us -> 78.6 us
    all_gather x1, waiting for transfers between devices: 35.8 us -> 7.23 us  [body(): lax.all_gather(expert_hidden, 'tp', axis=1, tiled=True)]
    ppermute x0 -> x15, starting transfers between devices: none -> 22.2 us  [the longest x7 14.1 us: gather_around(): upper.append(lax.ppermute(upper[-1] if upper else x, axis, back))]
    all_gather x1 -> x0, blocking collectives: 16.1 us -> none  [body(): lax.all_gather(shared_hidden, 'tp', axis=1, tiled=True)]
    all_to_all x2, waiting for transfers between devices: 0.01 us -> 11.2 us  [exchange_in_order(): lax.all_to_all(parts, axes[k], split_axis=k, concat_axis=k, tiled=True)]
    all_gather x1, waiting for transfers between devices: 9.08 us -> 14 us  [body(): lax.all_gather(conv_hidden, 'tp', axis=1, tiled=True)]
    ppermute x0 -> x15, waiting for transfers between devices: none -> 3.99 us  [the longest x8 2.39 us: gather_around(): lower.append(lax.ppermute(lower[-1] if lower else x, axis, pairs))]
  transfers between devices with their start and end apart: 6 -> 21, of which waited for: 4 -> 11; matrix products, arithmetic and copies ran while one was open for 6% -> 6% of each run, Pallas kernels for 0% -> 0%
where the time goes in v1:
time: 227 us; the launch traced here: 226 us
  waiting for transfers between devices  78.6 us (35%)
  blocking collectives  52.1 us (23%)
  starting transfers between devices  36.2 us (16%)
  local copies, waits for them, and re-layouts  24.2 us (11%)
  matrix products  14.2 us (6%)
  between operations  14.1 us (6%)
  other arithmetic  6.92 us (3%)
    all_gather x1, waiting for transfers between devices, body(): arrived = lax.all_gather(partial_rows, 'tp', axis=1, tiled=True)  42.1 us
    psum x1, blocking collectives, body(): lax.psum((jnp.sum(filtered, axis=1), jnp.sum(filtered * filtered, axis=1)...  27.3 us
    all_to_all x1, blocking collectives, body(): lax.all_to_all(own_slots, EP, split_axis=0, concat_axis=0, tiled=True)  24.8 us
    ppermute x7, starting transfers between devices, gather_around(): upper.append(lax.ppermute(upper[-1] if upper else x, axis, back))  14.1 us
    all_gather x1, waiting for transfers between devices, body(): lax.all_gather(conv_hidden, 'tp', axis=1, tiled=True)  14 us
    scatter x1, local copies, waits for them, and re-layouts, body(): outgoing = jnp.zeros((groups * capacity, model_width), jnp.bfloat16).at[s...  12.8 us
    all_to_all x2, waiting for transfers between devices, exchange_in_order(): lax.all_to_all(parts, axes[k], split_axis=k, concat_axis=k, tiled=True)  11.2 us
    all_to_all x2, starting transfers between devices, exchange_in_order(): lax.all_to_all(parts, axes[k], split_axis=k, concat_axis=k, tiled=True)  10.7 us
  transfers between devices with their start and end apart: 21, of which 11 were waited for; matrix products, arithmetic and copies ran while one was open for 6% of the time, Pallas kernels for 0%

profile of v1, /device:TPU:1, one launch (start us, length us, event | category | flops | bytes accessed | tf_op | source)
XLA Modules:
  0.0 226.2 jit_solution(13579544581368752729)
XLA Ops:
  7.2 0.0 all-gather.6.cloned.1.call-start
  7.2 0.9 copy.33
  8.1 0.1 eq.31
  8.2 0.1 eq.27
  8.3 0.7 broadcast_multiply_fusion
  9.0 1.2 fusion.6
  10.3 1.2 reduce-window.6
  11.4 0.2 slice_reduce_fusion
  11.7 0.1 copy.32
  11.8 0.1 mul.506
  11.9 1.2 fusion.8
  13.2 0.1 fusion.45
  13.3 12.8 %scatter_custom_fusion = bf16[1024,2048]{1,0:T(8,128)(2,1)} fusion(s32[512]{0:T(512)S(1)} %bitcast.155, bf16[128,2048]{1,0:T(8,128)(2,1)S(1)} %fusion.8, s32[1024]{0:T(1024)S(1)} %pad_clamp_fusion.2, bf16[]{:T(256)} %constant.63.clone.1), kind=kCustom, calls=%fused_computation.4 | custom fusion | bytes 4194306 | tf_op jit(solution)/shard_map/scatter | solution.py:126
  26.1 1.5 constant_dynamic-slice_fusion
  27.6 24.8 %all_to_all.15 = bf16[32,2,2048]{2,1,0:T(2,128)(2,1)S(1)} all-to-all(bf16[32,2,2048]{2,1,0:T(2,128)(2,1)S(1)} %constant_dynamic-slice_fusion), channel_id=1, replica_groups=mesh['ep_0'=8,'ep_1'=4,'tp'=16] {'ep_0','ep_1'}, dimensions={0} | all-to-all | bytes 524288 | tf_op jit(solution)/shard_map/all_to_all | solution.py:131
  52.4 0.8 copy.36
  53.2 0.0 all-gather.6.cloned.1.call-update
  53.3 0.0 all-gather.8.cloned.1.call-start
  53.3 42.1 %all-gather.6.cloned.1.call-done = bf16[32,32,2048]{2,0,1:T(8,128)(2,1)} async-done(((bf16[32,2,2048]{2,0,1:T(8,128)(2,1)}), bf16[32,32,2048]{2,0,1:T(8,128)(2,1)}) %all-gather.6.cloned.1.call-update) | async-done | bytes 4194320 | tf_op jit(solution)/shard_map/all_gather | solution.py:132
  95.4 4.5 %copy.37 = bf16[32,32,2048]{2,1,0:T(8,128)(2,1)S(1)} copy(bf16[32,32,2048]{2,0,1:T(8,128)(2,1)} %all-gather.6.cloned.1.call-done) | data formatting | bytes 8388608 | tf_op jit(solution)/shard_map/all_gather | solution.py:132
  99.9 1.3 fusion.11
  101.3 2.1 fusion.3
  103.4 0.0 all-gather.8.cloned.1.call-update
  103.5 0.0 all-gather.4.cloned.1.call-start
  103.5 0.3 fusion.50
  103.8 0.0 copy-done.5
  103.8 0.3 fusion.5
  104.1 1.2 collective-permute-start.1
  105.3 0.1 multiply_convert_fusion.1
  105.4 3.1 %collective-permute-start = (bf16[30,128]{1,0:T(8,128)(2,1)S(1)}, bf16[30,128]{1,0:T(8,128)(2,1)S(1)}, u32[]{:S(2)}, u32[]{:S(2)}) collective-permute-start(bf16[30,128]{1,0:T(8,128)(2,1)S(1)} %slice.262), channel_id=1, source_target_pairs={{0,16},{16,32},{32,48},{48,64},{64,80},{80,96},{96,112},{112,128},... | collective-permute-start | bytes 23048 | tf_op jit(solution)/shard_map/ppermute | solution.py:35
  108.6 2.0 collective-permute-start.2
  110.6 0.9 collective-permute-done.2
  111.5 2.1 collective-permute-start.3
  113.7 1.5 collective-permute-start.10
  115.2 0.6 collective-permute-done.3
  115.8 0.9 collective-permute-start.4
  116.8 2.8 %collective-permute-start.11 = (bf16[128,32]{0,1:T(8,128)(2,1)S(1)}, bf16[128,32]{0,1:T(8,128)(2,1)S(1)}, u32[]{:S(2)}, u32[]{:S(2)}) collective-permute-start(bf16[128,32]{0,1:T(8,128)(2,1)S(1)} %collective-permute-done.10), channel_id=1, source_target_pairs={{1,0},{2,1},{3,2},{4,3},{5,4},{6,5},{7,6},{8,7},{9,8},{10,9},{11,1... | collective-permute-start | bytes 24584 | tf_op jit(solution)/shard_map/ppermute | solution.py:25
  119.6 0.6 collective-permute-done.4
  120.1 0.1 copy.41
  120.2 0.3 collective-permute-done.11
  120.5 3.9 %collective-permute-start.12 = (bf16[128,32]{0,1:T(8,128)(2,1)S(1)}, bf16[128,32]{0,1:T(8,128)(2,1)S(1)}, u32[]{:S(2)}, u32[]{:S(2)}) collective-permute-start(bf16[128,32]{0,1:T(8,128)(2,1)S(1)} %collective-permute-done.11), channel_id=1, source_target_pairs={{1,0},{2,1},{3,2},{4,3},{5,4},{6,5},{7,6},{8,7},{9,8},{10,9},{11,1... | collective-permute-start | bytes 24584 | tf_op jit(solution)/shard_map/ppermute | solution.py:25
  124.4 0.3 collective-permute-done.5
  124.7 1.2 fusion.49
  125.9 27.3 %all-reduce = (f32[512]{0:T(512)S(1)}, f32[512]{0:T(512)S(1)}) all-reduce(f32[512]{0:T(512)S(1)} %get-tuple-element.3, f32[512]{0:T(512)S(1)} %get-tuple-element.2), channel_id=1, replica_groups=mesh['ep_0'=8,'ep_1'=4,'tp'=16] {'tp'}, use_global_device_ids=true, to_apply=%region_3.0 | all-reduce | flops 1024 | bytes 8192 | tf_op jit(solution)/shard_map/psum | solution.py:92
  153.2 3.8 %collective-permute-start.13 = (bf16[128,32]{0,1:T(8,128)(2,1)S(1)}, bf16[128,32]{0,1:T(8,128)(2,1)S(1)}, u32[]{:S(2)}, u32[]{:S(2)}) collective-permute-start(bf16[128,32]{0,1:T(8,128)(2,1)S(1)} %collective-permute-done.12), channel_id=1, source_target_pairs={{1,0},{2,1},{3,2},{4,3},{5,4},{6,5},{7,6},{8,7},{9,8},{10,9},{11,1... | collective-permute-start | bytes 24584 | tf_op jit(solution)/shard_map/ppermute | solution.py:25
  157.0 0.8 collective-permute-done.13
  157.8 0.5 collective-permute-start.14
  158.4 1.8 collective-permute-start.8
  160.2 0.9 multiply_convert_fusion
  161.1 0.0 all-gather.4.cloned.1.call-update
  161.1 0.5 collective-permute-done.14
  161.6 1.5 collective-permute-start.15
  163.3 7.2 %all-gather.8.cloned.1.call-done = bf16[1024,4096]{1,0:T(8,128)(2,1)} async-done(((bf16[1024,256]{1,0:T(8,128)(2,1)}), bf16[1024,4096]{1,0:T(8,128)(2,1)}) %all-gather.8.cloned.1.call-update) | async-done | bytes 8388624 | tf_op jit(solution)/shard_map/all_gather | solution.py:144
  170.5 6.4 %convolution_convert_fusion = bf16[1024,128]{1,0:T(8,128)(2,1)} fusion(bf16[1024,4096]{1,0:T(8,128)(2,1)} %all-gather.8.cloned.1.call-done, bf16[1,4096,128]{2,1,0:T(8,128)(2,1)S(1)} %copy-done.12), kind=kOutput, calls=%fused_computation.40 | convolution fusion | flops 1073872896 | bytes 9699328 | tf_op jit(solution)/shard_map/dot_general | solution.py:143
  176.9 5.7 %all-to-all-start.1 = ((bf16[8,4,1,32,128]{4,3,1,2,0:T(8,128)(2,1)}), bf16[8,4,1,32,128]{4,3,1,2,0:T(8,128)(2,1)S(1)}, u32[]{:S(2)}, u32[]{:S(2)}) async-start(bf16[8,4,1,32,128]{4,3,1,2,0:T(8,128)(2,1)} %bitcast.41), calls=%async_computation.1 | async-start | bytes 524288 | tf_op jit(solution)/shard_map/all_to_all | solution.py:53
  182.7 0.6 gather_fusion.1
  183.2 11.2 %all-to-all-done.1 = bf16[8,4,1,32,128]{4,3,1,2,0:T(8,128)(2,1)S(1)} async-done(((bf16[8,4,1,32,128]{4,3,1,2,0:T(8,128)(2,1)}), bf16[8,4,1,32,128]{4,3,1,2,0:T(8,128)(2,1)S(1)}, u32[]{:S(2)}, u32[]{:S(2)}) %all-to-all-start.1) | async-done | bytes 262176 | tf_op jit(solution)/shard_map/all_to_all | solution.py:53
  194.4 0.7 copy.39
  195.1 5.1 %all-to-all-start.2 = ((bf16[8,4,1,32,128]{4,3,0,2,1:T(8,128)(2,1)}), bf16[8,4,1,32,128]{4,3,0,2,1:T(8,128)(2,1)S(1)}, u32[]{:S(2)}, u32[]{:S(2)}) async-start(bf16[8,4,1,32,128]{4,3,0,2,1:T(8,128)(2,1)} %copy.39), calls=%async_computation.2 | async-start | bytes 524288 | tf_op jit(solution)/shard_map/all_to_all | solution.py:53
  200.2 14.0 %all-gather.4.cloned.1.call-done = bf16[512,2048]{1,0:T(8,128)(2,1)} async-done(((bf16[512,128]{1,0:T(8,128)(2,1)}), bf16[512,2048]{1,0:T(8,128)(2,1)}) %all-gather.4.cloned.1.call-update) | async-done | bytes 2097168 | tf_op jit(solution)/shard_map/all_gather | solution.py:103
  214.2 3.0 %convolution_convert_fusion.1 = bf16[512,128]{1,0:T(8,128)(2,1)} fusion(bf16[512,2048]{1,0:T(8,128)(2,1)} %all-gather.4.cloned.1.call-done, bf16[2048,128]{1,0:T(8,128)(2,1)S(1)} %copy-done.1), kind=kOutput, calls=%fused_computation.41 | convolution fusion | flops 268500992 | bytes 2752512 | tf_op jit(solution)/shard_map/dot_general | solution.py:102
  217.2 1.3 gather_fusion
  218.5 0.2 fusion.13
  218.8 0.8 fusion.4
  (70 shorter events, 0.4 us)
Async XLA Ops:
  7.2 92.8 %copy-start = (bf16[1,2048,256]{2,1,0:T(8,128)(2,1)S(1)}, bf16[1,2048,256]{2,1,0:T(8,128)(2,1)}, u32[]{:S(2)}) copy-start(bf16[1,2048,256]{2,1,0:T(8,128)(2,1)} %param.26) | copy-start | bytes 3145732
  7.2 88.3 %all-gather.6.cloned.1.call-start = ((), (), s32[]{:S(2)}) async-start(), calls=%async_computation.4 | async-start | bytes 4456448 | tf_op jit(solution)/shard_map/all_gather | solution.py:132
  53.3 117.3 %all-gather.8.cloned.1.call-start = ((), (), s32[]{:S(2)}) async-start(), calls=%async_computation.5 | async-start | bytes 8912896 | tf_op jit(solution)/shard_map/all_gather | solution.py:144
  99.9 1.3 copy-start.11
  101.2 2.3 %copy-start.4 = (bf16[2048,32]{0,1:T(8,128)(2,1)S(1)}, bf16[2048,32]{0,1:T(8,128)(2,1)}, u32[]{:S(2)}) copy-start(bf16[2048,32]{0,1:T(8,128)(2,1)} %param.29) | copy-start | bytes 393220
  101.2 2.6 %copy-start.5 = (bf16[2048,32]{0,1:T(8,128)(2,1)S(1)}, bf16[2048,32]{0,1:T(8,128)(2,1)}, u32[]{:S(2)}) copy-start(bf16[2048,32]{0,1:T(8,128)(2,1)} %param.30) | copy-start | bytes 393220
  101.2 4.1 %copy-start.2 = (bf16[512,128]{1,0:T(8,128)(2,1)S(1)}, bf16[512,128]{1,0:T(8,128)(2,1)}, u32[]{:S(2)}) copy-start(bf16[512,128]{1,0:T(8,128)(2,1)} %param.17) | copy-start | bytes 393220
  101.3 4.1 %copy-start.3 = (bf16[512,128]{1,0:T(8,128)(2,1)S(1)}, bf16[512,128]{1,0:T(8,128)(2,1)}, u32[]{:S(2)}) copy-start(bf16[512,128]{1,0:T(8,128)(2,1)} %param.16) | copy-start | bytes 393220
  101.3 7.2 %copy-start.7 = (f32[31,128]{1,0:T(8,128)S(1)}, f32[31,128]{1,0:T(8,128)}, u32[]{:S(2)}) copy-start(f32[31,128]{1,0:T(8,128)} %param.18) | copy-start | bytes 47620
  101.3 18.8 %copy-start.8 = (f32[128,4]{0,1:T(4,128)S(1)}, f32[128,4]{0,1:T(4,128)}, u32[]{:S(2)}) copy-start(f32[128,4]{0,1:T(4,128)} %param.25) | copy-start | bytes 6148
  101.3 58.9 %copy-start.9 = (f32[128]{0:T(128)S(1)}, f32[128]{0:T(128)}, u32[]{:S(2)}) copy-start(f32[128]{0:T(128)} %param.20) | copy-start | bytes 1540
  101.3 58.9 %copy-start.10 = (f32[128]{0:T(128)S(1)}, f32[128]{0:T(128)}, u32[]{:S(2)}) copy-start(f32[128]{0:T(128)} %param.19) | copy-start | bytes 1540
  101.3 69.2 %copy-start.12 = (bf16[1,4096,128]{2,1,0:T(8,128)(2,1)S(1)}, bf16[1,4096,128]{2,1,0:T(8,128)(2,1)}, u32[]{:S(2)}) copy-start(bf16[1,4096,128]{2,1,0:T(8,128)(2,1)} %param.28) | copy-start | bytes 3145732
  103.5 110.8 %all-gather.4.cloned.1.call-start = ((), (), s32[]{:S(2)}) async-start(), calls=%async_computation.3 | async-start | bytes 2228224 | tf_op jit(solution)/shard_map/all_gather | solution.py:103
  104.1 4.5 %collective-permute-start.1 = (bf16[128,32]{0,1:T(8,128)(2,1)S(1)}, bf16[128,32]{0,1:T(8,128)(2,1)S(1)}, u32[]{:S(2)}, u32[]{:S(2)}) collective-permute-start(bf16[128,32]{0,1:T(8,128)(2,1)S(1)} %fusion.5), channel_id=1, source_target_pairs={{0,1},{1,2},{2,3},{3,4},{4,5},{5,6},{6,7},{7,8},{8,9},{9,10},{10,1... | collective-permute-start | bytes 24584 | tf_op jit(solution)/shard_map/ppermute | solution.py:23
  105.3 8.4 %collective-permute-start.9 = (bf16[128,32]{0,1:T(8,128)(2,1)S(1)}, bf16[128,32]{0,1:T(8,128)(2,1)S(1)}, u32[]{:S(2)}, u32[]{:S(2)}) collective-permute-start(bf16[128,32]{0,1:T(8,128)(2,1)S(1)} %fusion.5), channel_id=1, source_target_pairs={{1,0},{2,1},{3,2},{4,3},{5,4},{6,5},{7,6},{8,7},{9,8},{10,9},{11,1... | collective-permute-start | bytes 24584 | tf_op jit(solution)/shard_map/ppermute | solution.py:25
  105.4 19.3 %collective-permute-start = (bf16[30,128]{1,0:T(8,128)(2,1)S(1)}, bf16[30,128]{1,0:T(8,128)(2,1)S(1)}, u32[]{:S(2)}, u32[]{:S(2)}) collective-permute-start(bf16[30,128]{1,0:T(8,128)(2,1)S(1)} %slice.262), channel_id=1, source_target_pairs={{0,16},{16,32},{32,48},{48,64},{64,80},{80,96},{96,112},{112,128},... | collective-permute-start | bytes 23048 | tf_op jit(solution)/shard_map/ppermute | solution.py:35
  108.6 3.0 %collective-permute-start.2 = (bf16[128,32]{0,1:T(8,128)(2,1)S(1)}, bf16[128,32]{0,1:T(8,128)(2,1)S(1)}, u32[]{:S(2)}, u32[]{:S(2)}) collective-permute-start(bf16[128,32]{0,1:T(8,128)(2,1)S(1)} %collective-permute-done.1), channel_id=1, source_target_pairs={{0,1},{1,2},{2,3},{3,4},{4,5},{5,6},{6,7},{7,8},{8,9},{9,10},{10,1... | collective-permute-start | bytes 24584 | tf_op jit(solution)/shard_map/ppermute | solution.py:23
  111.5 4.3 %collective-permute-start.3 = (bf16[128,32]{0,1:T(8,128)(2,1)S(1)}, bf16[128,32]{0,1:T(8,128)(2,1)S(1)}, u32[]{:S(2)}, u32[]{:S(2)}) collective-permute-start(bf16[128,32]{0,1:T(8,128)(2,1)S(1)} %collective-permute-done.2), channel_id=1, source_target_pairs={{0,1},{1,2},{2,3},{3,4},{4,5},{5,6},{6,7},{7,8},{8,9},{9,10},{10,1... | collective-permute-start | bytes 24584 | tf_op jit(solution)/shard_map/ppermute | solution.py:23
  113.7 3.1 %collective-permute-start.10 = (bf16[128,32]{0,1:T(8,128)(2,1)S(1)}, bf16[128,32]{0,1:T(8,128)(2,1)S(1)}, u32[]{:S(2)}, u32[]{:S(2)}) collective-permute-start(bf16[128,32]{0,1:T(8,128)(2,1)S(1)} %collective-permute-done.9), channel_id=1, source_target_pairs={{1,0},{2,1},{3,2},{4,3},{5,4},{6,5},{7,6},{8,7},{9,8},{10,9},{11,1... | collective-permute-start | bytes 24584 | tf_op jit(solution)/shard_map/ppermute | solution.py:25
  115.8 4.3 %collective-permute-start.4 = (bf16[128,32]{0,1:T(8,128)(2,1)S(1)}, bf16[128,32]{0,1:T(8,128)(2,1)S(1)}, u32[]{:S(2)}, u32[]{:S(2)}) collective-permute-start(bf16[128,32]{0,1:T(8,128)(2,1)S(1)} %collective-permute-done.3), channel_id=1, source_target_pairs={{0,1},{1,2},{2,3},{3,4},{4,5},{5,6},{6,7},{7,8},{8,9},{9,10},{10,1... | collective-permute-start | bytes 24584 | tf_op jit(solution)/shard_map/ppermute | solution.py:23
  116.8 3.8 %collective-permute-start.11 = (bf16[128,32]{0,1:T(8,128)(2,1)S(1)}, bf16[128,32]{0,1:T(8,128)(2,1)S(1)}, u32[]{:S(2)}, u32[]{:S(2)}) collective-permute-start(bf16[128,32]{0,1:T(8,128)(2,1)S(1)} %collective-permute-done.10), channel_id=1, source_target_pairs={{1,0},{2,1},{3,2},{4,3},{5,4},{6,5},{7,6},{8,7},{9,8},{10,9},{11,1... | collective-permute-start | bytes 24584 | tf_op jit(solution)/shard_map/ppermute | solution.py:25
  120.1 4.6 %collective-permute-start.5 = (bf16[128,32]{0,1:T(8,128)(2,1)S(1)}, bf16[128,32]{0,1:T(8,128)(2,1)S(1)}, u32[]{:S(2)}, u32[]{:S(2)}) collective-permute-start(bf16[128,32]{0,1:T(8,128)(2,1)S(1)} %collective-permute-done.4), channel_id=1, source_target_pairs={{0,1},{1,2},{2,3},{3,4},{4,5},{5,6},{6,7},{7,8},{8,9},{9,10},{10,1... | collective-permute-start | bytes 24584 | tf_op jit(solution)/shard_map/ppermute | solution.py:23
  120.5 32.7 %collective-permute-start.12 = (bf16[128,32]{0,1:T(8,128)(2,1)S(1)}, bf16[128,32]{0,1:T(8,128)(2,1)S(1)}, u32[]{:S(2)}, u32[]{:S(2)}) collective-permute-start(bf16[128,32]{0,1:T(8,128)(2,1)S(1)} %collective-permute-done.11), channel_id=1, source_target_pairs={{1,0},{2,1},{3,2},{4,3},{5,4},{6,5},{7,6},{8,7},{9,8},{10,9},{11,1... | collective-permute-start | bytes 24584 | tf_op jit(solution)/shard_map/ppermute | solution.py:25
  124.7 32.3 %collective-permute-start.6 = (bf16[128,32]{0,1:T(8,128)(2,1)S(1)}, bf16[128,32]{0,1:T(8,128)(2,1)S(1)}, u32[]{:S(2)}, u32[]{:S(2)}) collective-permute-start(bf16[128,32]{0,1:T(8,128)(2,1)S(1)} %collective-permute-done.5), channel_id=1, source_target_pairs={{0,1},{1,2},{2,3},{3,4},{4,5},{5,6},{6,7},{7,8},{8,9},{9,10},{10,1... | collective-permute-start | bytes 24584 | tf_op jit(solution)/shard_map/ppermute | solution.py:23
  153.2 4.6 %collective-permute-start.13 = (bf16[128,32]{0,1:T(8,128)(2,1)S(1)}, bf16[128,32]{0,1:T(8,128)(2,1)S(1)}, u32[]{:S(2)}, u32[]{:S(2)}) collective-permute-start(bf16[128,32]{0,1:T(8,128)(2,1)S(1)} %collective-permute-done.12), channel_id=1, source_target_pairs={{1,0},{2,1},{3,2},{4,3},{5,4},{6,5},{7,6},{8,7},{9,8},{10,9},{11,1... | collective-permute-start | bytes 24584 | tf_op jit(solution)/shard_map/ppermute | solution.py:25
  157.0 1.4 collective-permute-start.7
  157.8 3.8 %collective-permute-start.14 = (bf16[128,32]{0,1:T(8,128)(2,1)S(1)}, bf16[128,32]{0,1:T(8,128)(2,1)S(1)}, u32[]{:S(2)}, u32[]{:S(2)}) collective-permute-start(bf16[128,32]{0,1:T(8,128)(2,1)S(1)} %collective-permute-done.13), channel_id=1, source_target_pairs={{1,0},{2,1},{3,2},{4,3},{5,4},{6,5},{7,6},{8,7},{9,8},{10,9},{11,1... | collective-permute-start | bytes 24584 | tf_op jit(solution)/shard_map/ppermute | solution.py:25
  158.4 4.8 %collective-permute-start.8 = (bf16[128,32]{0,1:T(8,128)(2,1)S(1)}, bf16[128,32]{0,1:T(8,128)(2,1)S(1)}, u32[]{:S(2)}, u32[]{:S(2)}) collective-permute-start(bf16[128,32]{0,1:T(8,128)(2,1)S(1)} %collective-permute-done.7), channel_id=1, source_target_pairs={{0,1},{1,2},{2,3},{3,4},{4,5},{5,6},{6,7},{7,8},{8,9},{9,10},{10,1... | collective-permute-start | bytes 24584 | tf_op jit(solution)/shard_map/ppermute | solution.py:23
  161.6 21.0 %collective-permute-start.15 = (bf16[128,32]{0,1:T(8,128)(2,1)S(1)}, bf16[128,32]{0,1:T(8,128)(2,1)S(1)}, u32[]{:S(2)}, u32[]{:S(2)}) collective-permute-start(bf16[128,32]{0,1:T(8,128)(2,1)S(1)} %collective-permute-done.14), channel_id=1, source_target_pairs={{1,0},{2,1},{3,2},{4,3},{5,4},{6,5},{7,6},{8,7},{9,8},{10,9},{11,1... | collective-permute-start | bytes 24584 | tf_op jit(solution)/shard_map/ppermute | solution.py:25
  163.3 50.9 %copy-start.1 = (bf16[2048,128]{1,0:T(8,128)(2,1)S(1)}, bf16[2048,128]{1,0:T(8,128)(2,1)}, u32[]{:S(2)}) copy-start(bf16[2048,128]{1,0:T(8,128)(2,1)} %param.21) | copy-start | bytes 1572868
  176.9 41.8 %copy-start.6 = (bf16[512,128]{1,0:T(8,128)(2,1)S(1)}, bf16[512,128]{1,0:T(8,128)(2,1)}, u32[]{:S(2)}) copy-start(bf16[512,128]{1,0:T(8,128)(2,1)} %param.31) | copy-start | bytes 393220
  176.9 17.4 %all-to-all-start.1 = ((bf16[8,4,1,32,128]{4,3,1,2,0:T(8,128)(2,1)}), bf16[8,4,1,32,128]{4,3,1,2,0:T(8,128)(2,1)S(1)}, u32[]{:S(2)}, u32[]{:S(2)}) async-start(bf16[8,4,1,32,128]{4,3,1,2,0:T(8,128)(2,1)} %bitcast.41), calls=%async_computation.1 | async-start | bytes 524288 | tf_op jit(solution)/shard_map/all_to_all | solution.py:53
  195.1 22.1 %all-to-all-start.2 = ((bf16[8,4,1,32,128]{4,3,0,2,1:T(8,128)(2,1)}), bf16[8,4,1,32,128]{4,3,0,2,1:T(8,128)(2,1)S(1)}, u32[]{:S(2)}, u32[]{:S(2)}) async-start(bf16[8,4,1,32,128]{4,3,0,2,1:T(8,128)(2,1)} %copy.39), calls=%async_computation.2 | async-start | bytes 524288 | tf_op jit(solution)/shard_map/all_to_all | solution.py:53
Sparse Core Ops, SparseCore 0:
  53.4 42.0 all-gather.5
  103.6 66.9 all-gather.7
  173.1 41.0 all-gather.3
